TPU v7x, 128 devices: a whole 4x4x4 slice. The times are simulated.
128 devices in a mesh: ep: 32 (over z, y, core), tp: 4 (over x).
Axes of the slice: x: 4, y: 4, z: 4, core: 2. Of those that a mesh axis runs over, the one named last changes fastest.
Arguments:
- queries: bfloat16 [32768, 1024], P('ep', 'tp'), may hold values from -6 to 6
- key_rows: bfloat16 [32768, 256], P('ep', 'tp'), may hold values from -6 to 6
- values: bfloat16 [32768, 256], P('ep', 'tp'), may hold values from -6 to 6
- sink_logit: float32 [16], P('tp'), may hold values from 3 to 7
- out_weight: bfloat16 [1024, 2048], P('tp'), may hold values from -0.1875 to 0.1875
- out_gain: float32 [2048], replicated, may hold values from 0.1 to 1.9
- routed_tokens: bfloat16 [65536, 2048], P(('ep', 'tp')), may hold values from -6 to 6
- expert_ids: int32 [65536, 2], P(('ep', 'tp')), may hold values from 0 to 31, as said below
- route_weight: float32 [65536, 2], P(('ep', 'tp')), may hold values from 0.1 to 1
- routed_gain: float32 [2048], replicated, may hold values from 0.1 to 1.9
- expert_gate: bfloat16 [32, 2048, 1024], P('ep', None, 'tp'), may hold values from -0.125 to 0.125
- expert_up: bfloat16 [32, 2048, 1024], P('ep', None, 'tp'), may hold values from -0.125 to 0.125
- expert_down: bfloat16 [32, 2048, 1024], P('ep', None, 'tp'), may hold values from -0.1875 to 0.1875
Outputs:
- mixer_out: bfloat16 [32768, 2048], P(('ep', 'tp'))
- experts_out: bfloat16 [65536, 2048], P(('ep', 'tp'))
Inputs may be any that keep to these rules, and one draw needn't show every extreme that they name: `expert_ids`: both experts of a row lie in one group (equal id // 8); the 512 rows of one device name every group exactly 512 / 4 times; the rows of one device name no expert more than 64 times; in every device's rows some expert of each group is named exactly 64 times, and one expert is named exactly 64 times by the rows of every device.
All inputs are finite; a program needn't handle non-finite values.
Results may differ from a plain program's by a relative error of at most 0.0071.
Values may be sent and summed in bfloat16 or wider, within the bound.
No kernel may reach another device: no remote copies, remote signals or barrier semaphores. Data moves between devices by JAX's collectives and lax.ppermute only.
A program may use at most 128 MiB of HBM per device.

v0:
```python
import jax
import jax.numpy as jnp
from jax import lax
from jax.sharding import PartitionSpec as P

HEAD_DIM = 64
WINDOW = 128
QBLOCK = 512
EXPERTS = 32
TOP = 2
CAP = 64


epsilon = 1e-06


def padded(block, sides, width):
    for axis, dim in sides:
        count = lax.axis_size(axis)
        forward = [(i, i + 1) for i in range(count - 1)]
        backward = [(target, source) for source, target in forward]
        low = lax.ppermute(
            lax.slice_in_dim(block, block.shape[dim] - width, None, axis=dim), axis, forward
        )
        high = lax.ppermute(lax.slice_in_dim(block, 0, width, axis=dim), axis, backward)
        block = jnp.concatenate([low, block, high], axis=dim)
    return block


def local(
    queries,
    key_rows,
    values,
    sink_logit,
    out_weight,
    out_gain,
    routed_tokens,
    expert_ids,
    route_weight,
    routed_gain,
    expert_gate,
    expert_up,
    expert_down,
):
    row_count = queries.shape[0]
    heads_here = queries.shape[1] // HEAD_DIM
    kv_here = key_rows.shape[1] // HEAD_DIM
    group_size = heads_here // kv_here
    width = out_weight.shape[1]
    paired = jnp.concatenate((key_rows, values), axis=1)
    extended = padded(paired, (("ep", 0),), WINDOW)
    offset = lax.axis_index("ep") * row_count
    seq_total = row_count * lax.axis_size("ep")
    grouped = queries.reshape(row_count, kv_here, group_size, HEAD_DIM)
    sinks = sink_logit.reshape(kv_here, group_size)[:, :, None, None]
    span_keys = QBLOCK + 2 * WINDOW

    def attend_block(block_index):
        start_row = block_index * QBLOCK
        query_block = lax.dynamic_slice_in_dim(grouped, start_row, QBLOCK, 0)
        band = lax.dynamic_slice_in_dim(extended, start_row, span_keys, 0)
        key_block = band[:, : kv_here * HEAD_DIM].reshape(span_keys, kv_here, HEAD_DIM)
        value_block = band[:, kv_here * HEAD_DIM :].reshape(span_keys, kv_here, HEAD_DIM)
        scores = jnp.einsum(
            "qhgd,khd->hgqk", query_block, key_block, preferred_element_type=jnp.float32
        ) * HEAD_DIM ** (-0.5)
        query_pos = offset + start_row + jnp.arange(QBLOCK, dtype=jnp.int32)
        key_pos = offset + start_row - WINDOW + jnp.arange(span_keys, dtype=jnp.int32)
        valid = (
            (jnp.abs(key_pos[None, :] - query_pos[:, None]) <= WINDOW)
            & (key_pos[None, :] >= 0)
            & (key_pos[None, :] < seq_total)
        )
        masked = jnp.where(valid, scores, -1e30)
        largest = jnp.maximum(jnp.max(masked, axis=-1, keepdims=True), sinks)
        raised = jnp.where(valid, jnp.exp(masked - largest), 0.0)
        denominator = jnp.sum(raised, axis=-1, keepdims=True) + jnp.exp(sinks - largest)
        weights = (raised / denominator).astype(jnp.bfloat16)
        attended = jnp.einsum(
            "hgqk,khd->qhgd", weights, value_block, preferred_element_type=jnp.float32
        )
        return attended.astype(jnp.bfloat16).reshape(QBLOCK, heads_here * HEAD_DIM)

    attended = lax.map(attend_block, jnp.arange(row_count // QBLOCK, dtype=jnp.int32))
    attended = attended.reshape(row_count, heads_here * HEAD_DIM)
    mixed = lax.psum_scatter(
        jnp.dot(attended, out_weight, preferred_element_type=jnp.float32),
        "tp",
        scatter_dimension=0,
        tiled=True,
    )
    mixer_out = (
        mixed * lax.rsqrt(jnp.mean(mixed * mixed, axis=-1, keepdims=True) + epsilon) * out_gain
    ).astype(jnp.bfloat16)
    token_total = routed_tokens.shape[0]
    inputs = routed_tokens.astype(jnp.float32)
    normed = (
        inputs
        * lax.rsqrt(jnp.mean(inputs * inputs, axis=-1, keepdims=True) + epsilon)
        * routed_gain
    ).astype(jnp.bfloat16)
    flat_ids = expert_ids.reshape(-1)
    onehot = (flat_ids[:, None] == jnp.arange(EXPERTS, dtype=jnp.int32)[None, :]).astype(jnp.int32)
    earlier = jnp.cumsum(onehot, axis=0) - onehot
    slot_index = jnp.sum(earlier * onehot, axis=1)
    flat_dest = slot_index * EXPERTS + flat_ids
    source_rows = jnp.arange(token_total * TOP, dtype=jnp.int32) // TOP
    slot_token = jnp.full((CAP * EXPERTS,), token_total, jnp.int32).at[flat_dest].set(source_rows)
    outgoing = jnp.take(normed, slot_token, axis=0, mode="fill", fill_value=0).reshape(
        1, CAP, EXPERTS, width
    )
    arrived = lax.all_to_all(outgoing, "ep", split_axis=2, concat_axis=0, tiled=True)
    source_count, slot_count, local_experts, feature_count = arrived.shape
    rows_in = arrived.reshape(source_count * slot_count, local_experts, feature_count)
    gate_piece = lax.all_gather(expert_gate, "tp", axis=2, tiled=True)
    up_piece = lax.all_gather(expert_up, "tp", axis=2, tiled=True)
    down_piece = lax.all_gather(expert_down, "tp", axis=2, tiled=True)
    gate = jnp.einsum("red,edf->ref", rows_in, gate_piece, preferred_element_type=jnp.float32)
    upward = jnp.einsum("red,edf->ref", rows_in, up_piece, preferred_element_type=jnp.float32)
    hidden = (jax.nn.silu(gate) * upward).astype(jnp.bfloat16)
    summed = jnp.einsum("ref,edf->red", hidden, down_piece, preferred_element_type=jnp.float32)
    produced = summed.astype(jnp.bfloat16).reshape(
        source_count, slot_count, local_experts, feature_count
    )
    returned = lax.all_to_all(produced, "ep", split_axis=0, concat_axis=2, tiled=True)
    returned = returned.reshape(CAP * EXPERTS, width)
    picked_rows = jnp.take(returned, flat_dest, axis=0).reshape(token_total, TOP, width)
    experts_out = jnp.sum(
        picked_rows.astype(jnp.float32) * route_weight[:, :, None], axis=1
    ).astype(jnp.bfloat16)
    return (mixer_out, experts_out)


def solution(mesh):
    placed = (
        P("ep", "tp"),
        P("ep", "tp"),
        P("ep", "tp"),
        P("tp"),
        P("tp", None),
        P(),
        P(("ep", "tp"), None),
        P(("ep", "tp"), None),
        P(("ep", "tp"), None),
        P(),
        P("ep", None, "tp"),
        P("ep", None, "tp"),
        P("ep", None, "tp"),
    )
    return jax.shard_map(
        local,
        mesh=mesh,
        in_specs=placed,
        out_specs=(P(("ep", "tp"), None), P(("ep", "tp"), None)),
        check_vma=False,
    )
```

profile of v0, /device:TPU:0, one launch (start us, length us, event | category | flops | bytes accessed | tf_op | source)
XLA Modules:
  0.0 414.6 jit_solution(16288588751576607968)
XLA Ops:
  7.2 0.0 all-gather.4.cloned.1.call-start
  7.2 0.7 all-gather.4.cloned.1.call-update
  7.9 0.0 all-gather.6.cloned.1.call-start
  8.0 0.7 all-gather.6.cloned.1.call-update
  8.7 0.8 copy.50
  9.5 0.2 eq.29
  9.7 0.2 eq.25
  9.8 0.2 reshape.288
  10.0 9.0 %reduce-window.6 = s32[32,8,128]{2,1,0:T(8,128)S(1)} reduce-window(s32[32,8,128]{2,1,0:T(8,128)S(1)} %fusion.35, s32[]{:T(128)} %constant.129.clone.1), window={size=1x1x128 pad=0_0x0_0x127_0}, to_apply=%region_6.7 | reduce-window | flops 4161536 | bytes 262148 | tf_op jit(solution)/shard_map/reduce-window
  19.1 0.1 slice.34
  19.2 0.1 copy.52
  19.3 0.1 copy.53
  19.4 0.1 broadcast_add_fusion
  19.6 0.6 copy-done.6
  20.2 4.3 %scatter_custom_fusion = s32[2048]{0:T(1024)S(1)} fusion(s32[1024]{0:T(1024)S(1)} %bitcast.166, s32[1024]{0:T(1024)S(1)} %add_select_fusion, s32[]{:T(128)} %constant.140.clone.1), kind=kCustom, calls=%fused_computation.77 | custom fusion | bytes 8196 | tf_op jit(solution)/shard_map/scatter | solution.py:108
  24.5 0.1 broadcast_in_dim.74
  24.6 0.1 copy.57
  24.7 2.1 fusion.22
  26.9 2.2 fusion.24
  29.0 11.0 %gather_fusion = bf16[2048,2048]{1,0:T(8,128)(2,1)} fusion(bf16[512,2048]{1,0:T(8,128)(2,1)S(1)} %fusion.24, s32[2048]{0:T(1024)S(1)} %fusion.36), kind=kCustom, calls=%fused_computation | custom fusion | bytes 16785408 | tf_op jit(solution)/shard_map/jit(_take)/gather | solution.py:109
  40.0 16.8 %copy_select_fusion = bf16[1,64,32,2048]{3,1,0,2:T(8,128)(2,1)} fusion(bf16[1,64,32,2048]{3,2,1,0:T(8,128)(2,1)} %bitcast.155, pred[64,32]{0,1:T(8,128)(4,1)S(1)} %copy.57), kind=kLoop, calls=%fused_computation.37 | loop fusion | flops 4194304 | bytes 16779264 | tf_op jit(solution)/shard_map/jit(_take)/select_n | solution.py:109
  56.8 8.7 %all-to-all-start = ((bf16[1,64,32,2048]{3,1,0,2:T(8,128)(2,1)}), bf16[1,64,32,2048]{3,1,0,2:T(8,128)(2,1)}, u32[]{:S(2)}, u32[]{:S(2)}) async-start(bf16[1,64,32,2048]{3,1,0,2:T(8,128)(2,1)} %copy_select_fusion), calls=%async_computation.1 | async-start | bytes 16777216 | tf_op jit(solution)/shard_map/all_to_all | solution.py:112
  65.5 0.0 all-gather.8.cloned.1.call-start
  65.6 2.1 collective-permute-start
  67.7 1.3 collective-permute-start.1
  69.0 0.2 reduce-scatter.2.cloned.1.call-start
  69.3 1.3 copy.48
  70.6 1.4 collective-permute-done.1
  72.0 25.4 %while.12 = (s32[]{:T(128)}, bf16[2,512,256]{2,1,0:T(8,128)(2,1)S(1)}, s32[2]{0:T(128)S(1)}, bf16[1280,128]{0,1:T(8,128)(2,1)S(1)}, s32[]{:T(128)}, /*index=5*/b...) while((s32[]{:T(128)}, ...), condition=%wide.region_3.4_spmd, body=%wide.region_0.3_spmd.sunk | while | flops 426778112 | bytes 47478104 | solution.py:84
  72.0 0.6 dynamic_slice.28
  73.2 0.8 fusion.57
  74.0 1.2 fusion.58
  75.2 0.1 broadcast_maximum_fusion.2
  75.3 2.6 copy-done.2
  77.8 1.6 fusion.59
  79.4 0.1 exponential_add_fusion.2
  79.5 5.0 %fusion.60 = bf16[64,4,512]{2,0,1:T(8,128)(2,1)S(1)} fusion(f32[4,512]{1,0:T(4,128)S(1)} %exponential_add_fusion.2, f32[4,512]{1,0:T(4,128)S(1)} %broadcast_maximum_fusion.2, f32[768,512,4]{1,0,2:T(8,128)} %copy-done.2, pred[512,768]{0,1:T(8,128)(4,1)S(1)} %fusion.57, bf16[1280,128]{0,1:T(8,128)(2,1)S(1)} %get-tuple-element.194, s32[]{:T(128)S(6)} %select_n.125, ...), kind=kOutput, calls=%fused_computation.13.clone.1 | convolution fusion | flops 210894848 | bytes 7061512 | tf_op jit(solution)/shard_map/while/body/eval_jaxpr/hgqk,khd->qhgd/dot_general | solution.py:79
  84.5 0.1 copy.69
  84.7 0.6 dynamic_slice.28
  85.9 0.8 fusion.57
  86.6 1.2 fusion.58
  87.9 0.1 broadcast_maximum_fusion.2
  88.0 2.6 copy-done.2
  90.5 1.6 fusion.59
  92.1 0.1 exponential_add_fusion.2
  92.2 5.0 %fusion.60 = bf16[64,4,512]{2,0,1:T(8,128)(2,1)S(1)} fusion(f32[4,512]{1,0:T(4,128)S(1)} %exponential_add_fusion.2, f32[4,512]{1,0:T(4,128)S(1)} %broadcast_maximum_fusion.2, f32[768,512,4]{1,0,2:T(8,128)} %copy-done.2, pred[512,768]{0,1:T(8,128)(4,1)S(1)} %fusion.57, bf16[1280,128]{0,1:T(8,128)(2,1)S(1)} %get-tuple-element.194, s32[]{:T(128)S(6)} %select_n.125, ...), kind=kOutput, calls=%fused_computation.13.clone.1 | convolution fusion | flops 210894848 | bytes 7061512 | tf_op jit(solution)/shard_map/while/body/eval_jaxpr/hgqk,khd->qhgd/dot_general | solution.py:79
  97.2 0.1 copy.69
  97.4 4.5 %fusion.44 = f32[1024,2048]{1,0:T(8,128)} fusion(bf16[1024,256]{1,0:T(8,128)(2,1)S(1)} %bitcast.159, bf16[256,2048]{1,0:T(8,128)(2,1)S(1)} %copy-done), kind=kOutput, calls=%fused_computation.86 | convolution fusion | flops 1073741824 | bytes 9961472 | tf_op jit(solution)/shard_map/dot_general | solution.py:87
  101.9 0.0 all-gather.4.cloned.1.call-done
  102.0 69.7 %all-to-all-done = bf16[1,64,32,2048]{3,1,0,2:T(8,128)(2,1)} async-done(((bf16[1,64,32,2048]{3,1,0,2:T(8,128)(2,1)}), bf16[1,64,32,2048]{3,1,0,2:T(8,128)(2,1)}, u32[]{:S(2)}, u32[]{:S(2)}) %all-to-all-start) | async-done | bytes 8388640 | tf_op jit(solution)/shard_map/all_to_all | solution.py:112
  171.7 14.4 %fusion.29 = f32[2048,1024]{1,0:T(8,128)} fusion(bf16[2048,2048]{1,0:T(8,128)(2,1)} %bitcast.21, bf16[1,2048,1024]{2,1,0:T(8,128)(2,1)} %all-gather.4.cloned.1.call-done), kind=kOutput, calls=%fused_computation.49 | convolution fusion | flops 8589934592 | bytes 20971520 | tf_op jit(solution)/shard_map/red,edf->ref/dot_general | solution.py:118
  186.1 26.2 %convolution_convert_fusion = bf16[2048,2048]{1,0:T(8,128)(2,1)} fusion(bf16[1,2048,1024]{2,1,0:T(8,128)(2,1)} %all-gather.8.cloned.1.call-done, f32[2048,1024]{1,0:T(8,128)} %fusion.29, bf16[2048,2048]{1,0:T(8,128)(2,1)} %bitcast.21, bf16[1,2048,1024]{2,1,0:T(8,128)(2,1)} %all-gather.6.cloned.1.call-done), kind=kOutput, calls=%fused_computation.40 | convolution fusion | flops 17196646400 | bytes 33554432 | tf_op jit(solution)/shard_map/ref,edf->red/dot_general | solution.py:121
  212.3 33.3 %all-to-all-start.1 = ((bf16[32,64,1,2048]{3,1,2,0:T(8,128)(2,1)}), bf16[32,64,1,2048]{3,1,2,0:T(8,128)(2,1)}, u32[]{:S(2)}, u32[]{:S(2)}) async-start(bf16[32,64,1,2048]{3,1,2,0:T(8,128)(2,1)} %bitcast.156), calls=%async_computation.2 | async-start | bytes 16777216 | tf_op jit(solution)/shard_map/all_to_all | solution.py:125
  245.6 0.2 mul.111
  245.8 0.1 copy.54
  246.0 0.2 copy.55
  246.2 0.1 copy.61
  246.3 104.9 %all-to-all-done.1 = bf16[32,64,1,2048]{3,1,2,0:T(8,128)(2,1)} async-done(((bf16[32,64,1,2048]{3,1,2,0:T(8,128)(2,1)}), bf16[32,64,1,2048]{3,1,2,0:T(8,128)(2,1)}, u32[]{:S(2)}, u32[]{:S(2)}) %all-to-all-start.1) | async-done | bytes 8388640 | tf_op jit(solution)/shard_map/all_to_all | solution.py:125
  351.2 11.2 %copy.60 = bf16[1,64,32,1,2048]{4,2,1,3,0:T(8,128)(2,1)} copy(bf16[1,64,32,1,2048]{4,1,2,3,0:T(8,128)(2,1)} %bitcast.42) | data formatting | bytes 16777216 | tf_op jit(solution)/shard_map/all_to_all | solution.py:125
  362.4 13.3 %gather_fusion.1 = bf16[1024,2048]{1,0:T(8,128)(2,1)} fusion(bf16[2048,2048]{1,0:T(8,128)(2,1)} %bitcast.154, s32[1024]{0:T(1024)S(1)} %broadcast_clamp_fusion), kind=kCustom, calls=%fused_computation.1 | custom fusion | bytes 8392704 | tf_op jit(solution)/shard_map/jit(_take)/gather | solution.py:127
  375.7 7.7 %gather.15 = bf16[512,2,2048]{2,1,0:T(2,128)(2,1)} reshape(bf16[1024,2048]{1,0:T(8,128)(2,1)} %gather_fusion.1) | data formatting | bytes 8388608 | tf_op jit(solution)/shard_map/jit(_take)/gather | solution.py:127
  383.4 20.0 %multiply_reduce_fusion = bf16[512,2048]{1,0:T(8,128)(2,1)} fusion(bf16[512,2,2048]{2,1,0:T(2,128)(2,1)} %gather.15, pred[512,2]{1,0:T(8,128)(4,1)S(1)} %copy.55, f32[512,2]{1,0:T(8,128)S(1)} %copy.61), kind=kLoop, calls=%fused_computation.38 | loop fusion | flops 7340032 | bytes 6296576 | tf_op jit(solution)/shard_map/reduce_sum | solution.py:128
  403.5 1.8 multiply_reduce_fusion.1
  405.3 2.8 multiply_convert_fusion
  (60 shorter events, 0.4 us)
Async XLA Ops:
  7.2 90.2 %copy-start = (bf16[256,2048]{1,0:T(8,128)(2,1)S(1)}, bf16[256,2048]{1,0:T(8,128)(2,1)}, u32[]{:S(2)}) copy-start(bf16[256,2048]{1,0:T(8,128)(2,1)} %param.19) | copy-start | bytes 3145732
  7.2 19.7 %copy-start.11 = (f32[2048]{0:T(1024)S(1)}, f32[2048]{0:T(1024)}, u32[]{:S(2)}) copy-start(f32[2048]{0:T(1024)} %param.24) | copy-start | bytes 24580
  7.2 94.8 %all-gather.4.cloned.1.call-start = ((), (), s32[]{:S(2)}) async-start(), calls=%async_computation.4 | async-start | bytes 5242880 | tf_op jit(solution)/shard_map/all_gather | solution.py:115
  7.9 178.2 %all-gather.6.cloned.1.call-start = ((), (), s32[]{:S(2)}) async-start(), calls=%async_computation.5 | async-start | bytes 5242880 | tf_op jit(solution)/shard_map/all_gather | solution.py:116
  19.6 0.6 copy-start.6
  20.2 4.3 %copy-start.9 = (s32[1024,1]{0,1:T(1,128)}, s32[1024,1]{0,1:T(1,128)S(1)}, u32[]{:S(2)}) copy-start(s32[1024,1]{0,1:T(1,128)S(1)} %compare_select_fusion) | copy-start | bytes 12292
  56.8 8.8 %copy-start.3 = (bf16[1024,64]{0,1:T(8,128)(2,1)S(1)}, bf16[1024,64]{0,1:T(8,128)(2,1)}, u32[]{:S(2)}) copy-start(bf16[1024,64]{0,1:T(8,128)(2,1)} %param.16) | copy-start | bytes 393220
  56.8 8.8 %copy-start.4 = (bf16[1024,64]{0,1:T(8,128)(2,1)S(1)}, bf16[1024,64]{0,1:T(8,128)(2,1)}, u32[]{:S(2)}) copy-start(bf16[1024,64]{0,1:T(8,128)(2,1)} %param.17) | copy-start | bytes 393220
  56.8 15.2 %copy-start.5 = (f32[4]{0:T(128)S(1)}, f32[4]{0:T(128)}, u32[]{:S(2)}) copy-start(f32[4]{0:T(128)} %param.18) | copy-start | bytes 52
  56.8 114.9 %all-to-all-start = ((bf16[1,64,32,2048]{3,1,0,2:T(8,128)(2,1)}), bf16[1,64,32,2048]{3,1,0,2:T(8,128)(2,1)}, u32[]{:S(2)}, u32[]{:S(2)}) async-start(bf16[1,64,32,2048]{3,1,0,2:T(8,128)(2,1)} %copy_select_fusion), calls=%async_computation.1 | async-start | bytes 16777216 | tf_op jit(solution)/shard_map/all_to_all | solution.py:112
  65.5 120.6 %all-gather.8.cloned.1.call-start = ((), (), s32[]{:S(2)}) async-start(), calls=%async_computation.6 | async-start | bytes 5242880 | tf_op jit(solution)/shard_map/all_gather | solution.py:117
  65.6 4.9 %collective-permute-start = (bf16[128,128]{0,1:T(8,128)(2,1)S(1)}, bf16[128,128]{0,1:T(8,128)(2,1)S(1)}, u32[]{:S(2)}, u32[]{:S(2)}) collective-permute-start(bf16[128,128]{0,1:T(8,128)(2,1)S(1)} %get-tuple-element.110), channel_id=1, source_target_pairs={{0,4},{4,8},{8,12},{12,16},{16,20},{20,24},{24,28},{28,32},{32,36}... | collective-permute-start | bytes 98312 | tf_op jit(solution)/shard_map/ppermute | solution.py:22
  67.7 4.2 %collective-permute-start.1 = (bf16[128,128]{0,1:T(8,128)(2,1)S(1)}, bf16[128,128]{0,1:T(8,128)(2,1)S(1)}, u32[]{:S(2)}, u32[]{:S(2)}) collective-permute-start(bf16[128,128]{0,1:T(8,128)(2,1)S(1)} %get-tuple-element.111), channel_id=1, source_target_pairs={{4,0},{8,4},{12,8},{16,12},{20,16},{24,20},{28,24},{32,28},{36,32}... | collective-permute-start | bytes 98312 | tf_op jit(solution)/shard_map/ppermute | solution.py:25
  69.0 334.4 %reduce-scatter.2.cloned.1.call-start = ((), (), s32[]{:S(2)}) async-start(), calls=%async_computation.3 | async-start | bytes 10485760 | tf_op jit(solution)/shard_map/reduce_scatter | solution.py:86
  75.2 2.7 copy-start.2
  87.9 2.7 copy-start.2
  212.3 33.3 %copy-start.7 = (s32[1024]{0:T(1024)S(1)}, s32[1024]{0:T(1024)}, u32[]{:S(2)}) copy-start(s32[1024]{0:T(1024)} %copy-done.6) | copy-start | bytes 12292
  212.3 33.6 %copy-start.8 = (s32[512,2]{0,1:T(2,128)S(1)}, s32[512,2]{0,1:T(2,128)}, u32[]{:S(2)}) copy-start(s32[512,2]{0,1:T(2,128)} %param.22) | copy-start | bytes 12292
  212.3 33.8 %copy-start.13 = (f32[512,2]{0,1:T(2,128)S(1)}, f32[512,2]{0,1:T(2,128)}, u32[]{:S(2)}) copy-start(f32[512,2]{0,1:T(2,128)} %param.23) | copy-start | bytes 12292
  212.3 34.0 %copy-start.10 = (s32[1024,1]{0,1:T(1,128)S(1)}, s32[1024,1]{0,1:T(1,128)}, u32[]{:S(2)}) copy-start(s32[1024,1]{0,1:T(1,128)} %copy-done.9) | copy-start | bytes 12292
  212.3 138.9 %all-to-all-start.1 = ((bf16[32,64,1,2048]{3,1,2,0:T(8,128)(2,1)}), bf16[32,64,1,2048]{3,1,2,0:T(8,128)(2,1)}, u32[]{:S(2)}, u32[]{:S(2)}) async-start(bf16[32,64,1,2048]{3,1,2,0:T(8,128)(2,1)} %bitcast.156), calls=%async_computation.2 | async-start | bytes 16777216 | tf_op jit(solution)/shard_map/all_to_all | solution.py:125
  375.7 32.4 %copy-start.1 = (bf16[256,2048]{1,0:T(8,128)(2,1)S(1)}, bf16[256,2048]{1,0:T(8,128)(2,1)}, u32[]{:S(2)}) copy-start(bf16[256,2048]{1,0:T(8,128)(2,1)} %param.19) | copy-start | bytes 3145732
  383.4 21.9 %copy-start.12 = (f32[2048]{0:T(1024)S(1)}, f32[2048]{0:T(1024)}, u32[]{:S(2)}) copy-start(f32[2048]{0:T(1024)} %param.20) | copy-start | bytes 24580
Sparse Core Ops, SparseCore 0:
  9.7 53.8 all-gather.3
  65.2 52.2 all-gather.5
  119.2 52.2 all-gather.7
  173.9 105.0 reduce-scatter.1
where the time goes:
time: 416 us; the launch traced here: 415 us
  waiting for transfers between devices  177 us (43%)
  other arithmetic  60 us (14%)
  local copies, waits for them, and re-layouts  58.5 us (14%)
  matrix products  57.6 us (14%)
  starting transfers between devices  45.7 us (11%)
  between operations  14.1 us (3%)
    all_to_all x1, waiting for transfers between devices, local(): lax.all_to_all(produced, 'ep', split_axis=0, concat_axis=2, tiled=True)  105 us
    all_to_all x1, waiting for transfers between devices, local(): lax.all_to_all(outgoing, 'ep', split_axis=2, concat_axis=0, tiled=True)  69.7 us
    all_to_all x1, starting transfers between devices, local(): lax.all_to_all(produced, 'ep', split_axis=0, concat_axis=2, tiled=True)  33.3 us
    dot_general x1, matrix products, local(): jnp.einsum('ref,edf->red', hidden, down_piece, preferred_element_type=jnp...  26.2 us
    gather x2, local copies, waits for them, and re-layouts, local(): jnp.take(returned, flat_dest, axis=0).reshape(token_total, TOP, width)  21 us
    reduce_sum x1, other arithmetic, local(): jnp.sum(picked_rows.astype(jnp.float32) * route_weight[:, :, None], axis=1)  20 us
    select_n x1, other arithmetic, local(): jnp.take(normed, slot_token, axis=0, mode='fill', fill_value=0)  16.8 us
    dot_general x1, matrix products, local(): jnp.einsum('red,edf->ref', rows_in, gate_piece, preferred_element_type=jn...  14.4 us
  transfers between devices with their start and end apart: 8, of which 3 were waited for; matrix products, arithmetic and copies ran while one was open for 40% of the time, Pallas kernels for 0%

commit v1 on v0

v1 whole, which is shorter than its diff:
```python
import functools

import jax
import jax.numpy as jnp
from jax import lax
from jax.experimental import pallas as pl
from jax.experimental.pallas import tpu as pltpu
from jax.sharding import Mesh, PartitionSpec as P

HEAD_DIM = 64
WINDOW = 128
QBLOCK = 512
CAP = 64
GROUPS = 4
META = 128
STEP_BLOCKS = 8

epsilon = 1e-06
f32 = jnp.float32
bf16 = jnp.bfloat16
NT = (((1,), (1,)), ((), ()))
TN = (((0,), (0,)), ((), ()))
VMEM_LIMIT = 60 * 1024 * 1024


def shifted(size, shift):
    return [(i, (i + shift) % size) for i in range(size)]


def iota(shape, dim, kind=jnp.int32):
    return lax.broadcasted_iota(jnp.int32, shape, dim).astype(kind)


def prep_kernel(place, tok, ids_t, weight_t, gain, first, second, third, fourth, order):
    count = tok.shape[0]
    each = count // GROUPS
    inputs = tok[...].astype(f32)
    scale = lax.rsqrt(jnp.mean(inputs * inputs, axis=-1, keepdims=True) + epsilon)
    normed = (inputs * scale * gain[...]).astype(bf16)
    ids = ids_t[...]
    group = lax.shift_right_logical(ids[0:1, :], 3)
    relative = lax.bitwise_and(group - place[0] + GROUPS, GROUPS - 1)
    member = (iota((16, count), 0) == relative).astype(f32)
    before = (iota((count, count), 0) < iota((count, count), 1)).astype(f32).astype(bf16)
    earlier = jnp.dot(member.astype(bf16), before, preferred_element_type=f32)
    rank = jnp.sum(earlier * member, axis=0, keepdims=True)
    slot = (relative * each).astype(f32) + rank
    permute = (iota((count, count), 0, f32) == slot).astype(f32).astype(bf16)
    order[...] = permute
    rows = jnp.dot(permute, normed, preferred_element_type=f32).astype(bf16)
    line = iota((META, count), 0)
    meta = jnp.where(line == 0, ids[0:1, :].astype(f32), 0.0)
    meta = jnp.where(line == 1, ids[1:2, :].astype(f32), meta)
    for k in range(2):
        rest = weight_t[k : k + 1, :]
        for part in range(3):
            piece = rest.astype(bf16).astype(f32)
            meta = jnp.where(line == 2 + 3 * k + part, piece, meta)
            rest = rest - piece
    tags = lax.dot_general(permute, meta.astype(bf16), NT, preferred_element_type=f32).astype(bf16)
    width = tok.shape[1]
    for index, out in enumerate((first, second, third, fourth)):
        out[:, :width] = rows[index * each : (index + 1) * each]
        out[:, width:] = tags[index * each : (index + 1) * each]


def prepare(place, tokens, ids, weights, gain):
    count, width = tokens.shape
    chunk = jax.ShapeDtypeStruct((count // GROUPS, width + META), bf16)
    vmem = pl.BlockSpec(memory_space=pltpu.VMEM)
    return pl.pallas_call(
        prep_kernel,
        out_shape=(chunk, chunk, chunk, chunk, jax.ShapeDtypeStruct((count, count), bf16)),
        in_specs=[pl.BlockSpec(memory_space=pltpu.SMEM)] + [vmem] * 4,
        out_specs=(vmem,) * 5,
        compiler_params=pltpu.CompilerParams(vmem_limit_bytes=VMEM_LIMIT),
        cost_estimate=pl.CostEstimate(flops=6_000_000_000, bytes_accessed=6_000_000, transcendentals=512),
        name="prep",
    )(place, tokens, ids.T, weights.T, gain.reshape(1, width))


def choices(tags, expert):
    blocks = tags.shape[0]
    size = tags.shape[1]
    lines = [jnp.transpose(tags[b].astype(f32)) for b in range(blocks)]
    hits = [tuple((t[k : k + 1] == expert).astype(f32) for k in range(2)) for t in lines]
    row = iota((16, size), 0)
    counts = jnp.zeros((16, size), f32)
    for b in range(blocks):
        counts = jnp.where(row == b, hits[b][0] + hits[b][1], counts)
    before = (iota((size, size), 0) < iota((size, size), 1)).astype(f32).astype(bf16)
    earlier = jnp.dot(counts.astype(bf16), before, preferred_element_type=f32)
    place = iota((2 * CAP, size), 0, f32)
    found = []
    for pair in range(blocks // 2):
        halves = []
        weight = jnp.zeros((2 * CAP, size), f32)
        for j in range(2):
            b = 2 * pair + j
            slot = earlier[b : b + 1] + float(CAP * j)
            one = jnp.where(place == slot, hits[b][0], 0.0)
            two = jnp.where(place == slot + hits[b][0], hits[b][1], 0.0)
            halves.append(one + two)
            t = lines[b]
            weight = weight + one * (t[2:3] + t[3:4] + t[4:5]) + two * (t[5:6] + t[6:7] + t[7:8])
        pick = jnp.concatenate(halves, axis=1).astype(bf16)
        found.append((pick, jnp.sum(weight, axis=1, keepdims=True)))
    return found


def hidden_kernel(place, tok, *refs):
    gates, ups, out, rows = refs[:4], refs[4:8], refs[8], refs[9]
    width = gates[0].shape[0]
    expert = place[1].astype(f32)
    size = tok.shape[1]
    for pair, (pick, _) in enumerate(choices(tok[:, :, width:], expert)):
        both = tok[2 * pair : 2 * pair + 2, :, :width].reshape(2 * size, width)
        rows[2 * CAP * pair : 2 * CAP * (pair + 1)] = jnp.dot(pick, both, preferred_element_type=f32).astype(bf16)
    inputs = rows[...]
    wide = gates[0].shape[1]
    for s in range(4):
        gate = jnp.dot(inputs, gates[s][...], preferred_element_type=f32)
        up = jnp.dot(inputs, ups[s][...], preferred_element_type=f32)
        out[:, s * wide : (s + 1) * wide] = (gate / (1.0 + jnp.exp(-gate)) * up).astype(bf16)


def hidden_units(place, tokens, gates, ups):
    blocks, size, full = tokens.shape
    width, wide = gates[0].shape
    steps = blocks // STEP_BLOCKS
    rows = STEP_BLOCKS * CAP
    weight = pl.BlockSpec((width, wide), lambda i: (0, 0))
    return pl.pallas_call(
        hidden_kernel,
        grid=(steps,),
        out_shape=jax.ShapeDtypeStruct((blocks * CAP, 4 * wide), bf16),
        in_specs=[
            pl.BlockSpec(memory_space=pltpu.SMEM),
            pl.BlockSpec((STEP_BLOCKS, size, full), lambda i: (i, 0, 0)),
        ]
        + [weight] * 8,
        out_specs=pl.BlockSpec((rows, 4 * wide), lambda i: (i, 0)),
        scratch_shapes=[pltpu.VMEM((rows, width), bf16)],
        compiler_params=pltpu.CompilerParams(vmem_limit_bytes=VMEM_LIMIT),
        cost_estimate=pl.CostEstimate(
            flops=blocks * CAP * width * wide * 16, bytes_accessed=blocks * size * full * 2 + 8_000_000, transcendentals=0
        ),
        name="hidden",
    )(place, tokens, *gates, *ups)


def result_kernel(place, tags, hidden, *refs):
    downs, out = refs[:5], refs[5]
    wide = downs[0].shape[1]
    size = tags.shape[1]
    expert = place[1].astype(f32)
    half = downs[3].shape[0]
    found = choices(tags[...], expert)
    units = [hidden[:, s * wide : (s + 1) * wide] for s in range(4)]
    for part in range(2):
        cols = slice(part * half, (part + 1) * half)
        total = lax.dot_general(units[3], downs[3 + part][...], NT, preferred_element_type=f32)
        for s in range(3):
            total = total + lax.dot_general(units[s], downs[s][cols, :], NT, preferred_element_type=f32)
        result = total.astype(bf16).astype(f32)
        for pair, (pick, weight) in enumerate(found):
            scaled = (result[2 * CAP * pair : 2 * CAP * (pair + 1)] * weight).astype(bf16)
            spread = lax.dot_general(pick, scaled, TN, preferred_element_type=f32)
            out[2 * size * pair : 2 * size * (pair + 1), cols] = spread.astype(bf16)


def results(place, tokens, hidden, downs):
    blocks, size, full = tokens.shape
    wide = downs[0].shape[1]
    width = downs[0].shape[0]
    steps = blocks // STEP_BLOCKS
    rows = STEP_BLOCKS * CAP
    return pl.pallas_call(
        result_kernel,
        grid=(steps,),
        out_shape=jax.ShapeDtypeStruct((blocks * size, width), bf16),
        in_specs=[
            pl.BlockSpec(memory_space=pltpu.SMEM),
            pl.BlockSpec((STEP_BLOCKS, size, META), lambda i: (i, 0, width // META)),
            pl.BlockSpec((rows, 4 * wide), lambda i: (i, 0)),
        ]
        + [pl.BlockSpec(d.shape, lambda i: (0, 0)) for d in downs],
        out_specs=pl.BlockSpec((STEP_BLOCKS * size, width), lambda i: (i, 0)),
        compiler_params=pltpu.CompilerParams(vmem_limit_bytes=VMEM_LIMIT),
        cost_estimate=pl.CostEstimate(
            flops=blocks * CAP * width * wide * 12, bytes_accessed=blocks * size * width * 2 + 8_000_000, transcendentals=0
        ),
        name="result",
    )(place, tokens, hidden, *downs)


def finish_kernel(order, first, second, third, fourth, out):
    each = first.shape[0]
    total = jnp.zeros(out.shape, f32)
    for index, piece in enumerate((first, second, third, fourth)):
        total = total + lax.dot_general(
            order[index * each : (index + 1) * each, :], piece[...], TN, preferred_element_type=f32
        )
    out[...] = total.astype(bf16)


def finish(order, pieces):
    count = order.shape[0]
    width = pieces[0].shape[1]
    vmem = pl.BlockSpec(memory_space=pltpu.VMEM)
    return pl.pallas_call(
        finish_kernel,
        out_shape=jax.ShapeDtypeStruct((count, width), bf16),
        in_specs=[vmem] * 5,
        out_specs=vmem,
        compiler_params=pltpu.CompilerParams(vmem_limit_bytes=VMEM_LIMIT),
        cost_estimate=pl.CostEstimate(flops=2_000_000_000, bytes_accessed=5_000_000, transcendentals=0),
        name="finish",
    )(order, *pieces)


def ring_weights(gate, up, down):
    right = lambda v: lax.ppermute(v, "x", shifted(4, 1))
    left = lambda v: lax.ppermute(v, "x", shifted(4, -1))
    half = down.shape[0] // 2
    gate_low, up_low = right(gate), right(up)
    gate_high, up_high = left(gate), left(up)
    down_low, down_high = right(down), left(down)
    gate_far = right(gate_low)
    up_far = left(up_high)
    down_far = right(down_low[:half]), left(down_high[half:])
    return (
        (gate, gate_low, gate_high, gate_far),
        (up, up_low, up_high, up_far),
        (down, down_low, down_high) + down_far,
    )


def padded(block, width):
    axes = ("z", "y", "c")
    count = 1
    for axis in axes:
        count *= lax.axis_size(axis)
    forward = [(i, i + 1) for i in range(count - 1)]
    backward = [(target, source) for source, target in forward]
    low = lax.ppermute(block[-width:], axes, forward)
    high = lax.ppermute(block[:width], axes, backward)
    return jnp.concatenate([low, block, high], axis=0)


def attention(queries, key_rows, values, sink_logit, offset, seq_total):
    row_count = queries.shape[0]
    heads_here = queries.shape[1] // HEAD_DIM
    kv_here = key_rows.shape[1] // HEAD_DIM
    group_size = heads_here // kv_here
    extended = padded(jnp.concatenate((key_rows, values), axis=1), WINDOW)
    grouped = queries.reshape(row_count, kv_here, group_size, HEAD_DIM)
    sinks = sink_logit.reshape(kv_here, group_size)[:, :, None, None]
    span_keys = QBLOCK + 2 * WINDOW

    def attend_block(block_index):
        start_row = block_index * QBLOCK
        query_block = lax.dynamic_slice_in_dim(grouped, start_row, QBLOCK, 0)
        band = lax.dynamic_slice_in_dim(extended, start_row, span_keys, 0)
        key_block = band[:, : kv_here * HEAD_DIM].reshape(span_keys, kv_here, HEAD_DIM)
        value_block = band[:, kv_here * HEAD_DIM :].reshape(span_keys, kv_here, HEAD_DIM)
        scores = jnp.einsum("qhgd,khd->hgqk", query_block, key_block, preferred_element_type=f32) * HEAD_DIM ** (-0.5)
        query_pos = offset + start_row + jnp.arange(QBLOCK, dtype=jnp.int32)
        key_pos = offset + start_row - WINDOW + jnp.arange(span_keys, dtype=jnp.int32)
        valid = (
            (jnp.abs(key_pos[None, :] - query_pos[:, None]) <= WINDOW)
            & (key_pos[None, :] >= 0)
            & (key_pos[None, :] < seq_total)
        )
        masked = jnp.where(valid, scores, -1e30)
        largest = jnp.maximum(jnp.max(masked, axis=-1, keepdims=True), sinks)
        raised = jnp.where(valid, jnp.exp(masked - largest), 0.0)
        denominator = jnp.sum(raised, axis=-1, keepdims=True) + jnp.exp(sinks - largest)
        weights = (raised / denominator).astype(bf16)
        attended = jnp.einsum("hgqk,khd->qhgd", weights, value_block, preferred_element_type=f32)
        return attended.astype(bf16).reshape(QBLOCK, heads_here * HEAD_DIM)

    attended = lax.map(attend_block, jnp.arange(row_count // QBLOCK, dtype=jnp.int32))
    return attended.reshape(row_count, heads_here * HEAD_DIM)


def local(
    queries,
    key_rows,
    values,
    sink_logit,
    out_weight,
    out_gain,
    routed_tokens,
    expert_ids,
    route_weight,
    routed_gain,
    expert_gate,
    expert_up,
    expert_down,
):
    row_count = queries.shape[0]
    z, y, c = lax.axis_index("z"), lax.axis_index("y"), lax.axis_index("c")
    expert = (z * 4 + y) * 2 + c
    place = jnp.stack([z, expert]).astype(jnp.int32)
    plane = ("y", "c")
    gates, ups, downs = ring_weights(expert_gate[0], expert_up[0], expert_down[0])

    chunks = prepare(place, routed_tokens, expert_ids, route_weight, routed_gain)
    own, order = chunks[0], chunks[4]
    moved = [lax.ppermute(chunks[s], "z", shifted(4, s)) for s in (1, 3, 2)]
    near = lax.all_gather(own, plane, axis=0, tiled=False)
    far = lax.all_gather(jnp.concatenate(moved, axis=0), plane, axis=0, tiled=False)
    size, full = own.shape
    near = near.reshape(8, size, full)
    far = far.reshape(24, size, full)

    attended = attention(queries, key_rows, values, sink_logit, expert * row_count, row_count * 32)
    quarter = row_count // 4
    heads = attended.shape[1]
    crossed = lax.all_to_all(attended.reshape(4, quarter, heads), "x", 0, 0)
    low = lax.ppermute(out_weight, "x", shifted(4, 1))
    high = lax.ppermute(out_weight, "x", shifted(4, -1))
    half = heads // 2
    across = lax.ppermute(low[:half], "x", shifted(4, 1)), lax.ppermute(high[half:], "x", shifted(4, -1))
    across = jnp.concatenate(across, axis=0)
    x = lax.axis_index("x")
    mixed = jnp.zeros((quarter, out_weight.shape[1]), f32)
    for shift, piece in ((0, out_weight), (3, low), (1, high), (2, across)):
        part = lax.dynamic_index_in_dim(crossed, (x + shift) % 4, 0, keepdims=False)
        mixed = mixed + jnp.dot(part, piece, preferred_element_type=f32)
    mixer_out = (
        mixed * lax.rsqrt(jnp.mean(mixed * mixed, axis=-1, keepdims=True) + epsilon) * out_gain
    ).astype(bf16)

    near_hidden = hidden_units(place, near, gates, ups)
    far_hidden = hidden_units(place, far, gates, ups)
    far_part = results(place, far, far_hidden, downs)
    near_part = results(place, near, near_hidden, downs)
    far_sum = lax.psum_scatter(far_part, plane, scatter_dimension=0, tiled=True)
    near_sum = lax.psum_scatter(near_part, plane, scatter_dimension=0, tiled=True)
    back = {0: near_sum}
    for index, s in enumerate((1, 3, 2)):
        back[s] = lax.ppermute(far_sum[index * size : (index + 1) * size], "z", shifted(4, -s))
    experts_out = finish(order, [back[s] for s in range(4)])
    return (mixer_out, experts_out)


def solution(mesh):
    split = Mesh(mesh.devices.reshape(4, 4, 2, 4), ("z", "y", "c", "x"))
    ep = ("z", "y", "c")
    placed = (
        P(ep, "x"),
        P(ep, "x"),
        P(ep, "x"),
        P("x"),
        P("x", None),
        P(),
        P(ep + ("x",), None),
        P(ep + ("x",), None),
        P(ep + ("x",), None),
        P(),
        P(ep, None, "x"),
        P(ep, None, "x"),
        P(ep, None, "x"),
    )
    return jax.shard_map(
        local,
        mesh=split,
        in_specs=placed,
        out_specs=(P(ep + ("x",), None), P(ep + ("x",), None)),
        check_vma=False,
    )
```

time: 416 us -> 306 us (0.74)
  Pallas kernels: 0 us -> 68.1 us
  other arithmetic: 60 us -> 8.16 us
  local copies, waits for them, and re-layouts: 58.5 us -> 14.4 us
  matrix products: 57.6 us -> 19.1 us
  waiting for transfers between devices: 177 us -> 142 us
  starting transfers between devices: 45.7 us -> 38.5 us
    all_to_all x2 -> x1, waiting for transfers between devices: 175 us -> 6.37 us  [local(): crossed = lax.all_to_all(attended.reshape(4, quarter, heads), 'x', 0, 0)]
    ppermute x2 -> x22, waiting for transfers between devices: 1.4 us -> 110 us  [the longest x5 60.6 us: ring_weights(): right = lambda v: lax.ppermute(v, 'x', shifted(4, 1))]
    pallas_call x0 -> x6, Pallas kernels: none -> 68.1 us  [the longest x2 33.9 us: hidden_units(): pl.pallas_call(hidden_kernel, grid=(steps,), out_shape=jax.ShapeDtypeStru...]
    dot_general x3 -> x4, matrix products: 45.1 us -> 6.58 us  [local(): mixed = mixed + jnp.dot(part, piece, preferred_element_type=f32)]
    all_to_all x2 -> x1, starting transfers between devices: 42 us -> 4.28 us  [local(): crossed = lax.all_to_all(attended.reshape(4, quarter, heads), 'x', 0, 0)]
    gather x3 -> x0, local copies, waits for them, and re-layouts: 32 us -> none  [the longest x2 21 us: local(): jnp.take(returned, flat_dest, axis=0).reshape(token_total, TOP, width)]
    ppermute x2 -> x22, starting transfers between devices: 3.4 us -> 34.1 us  [the longest x5 9.53 us: ring_weights(): left = lambda v: lax.ppermute(v, 'x', shifted(4, -1))]
    reduce_scatter x1 -> x2, waiting for transfers between devices: 0.01 us -> 24.8 us  [the longest x1 24.7 us: local(): lax.psum_scatter(near_part, plane, scatter_dimension=0, tiled=True)]
  transfers between devices with their start and end apart: 8 -> 27, of which waited for: 3 -> 10; matrix products, arithmetic and copies ran while one was open for 40% -> 11% of each run, Pallas kernels for 0% -> 19%
where the time goes in v1:
time: 306 us; the launch traced here: 305 us
  waiting for transfers between devices  142 us (46%)
  Pallas kernels  68.1 us (22%)
  starting transfers between devices  38.5 us (13%)
  matrix products  19.1 us (6%)
  local copies, waits for them, and re-layouts  14.4 us (5%)
  between operations  14 us (5%)
  other arithmetic  8.16 us (3%)
    ppermute x5, waiting for transfers between devices, ring_weights(): right = lambda v: lax.ppermute(v, 'x', shifted(4, 1))  60.6 us
    pallas_call x2, Pallas kernels, hidden_units(): pl.pallas_call(hidden_kernel, grid=(steps,), out_shape=jax.ShapeDtypeStru...  33.9 us
    reduce_scatter x1, waiting for transfers between devices, local(): lax.psum_scatter(near_part, plane, scatter_dimension=0, tiled=True)  24.7 us
    pallas_call x2, Pallas kernels, results(): pl.pallas_call(result_kernel, grid=(steps,), out_shape=jax.ShapeDtypeStru...  23.6 us
    ppermute x3, waiting for transfers between devices, local(): moved = [lax.ppermute(chunks[s], 'z', shifted(4, s)) for s in (1, 3, 2)]  23.5 us
    ppermute x5, waiting for transfers between devices, ring_weights(): left = lambda v: lax.ppermute(v, 'x', shifted(4, -1))  19.1 us
    dot_general x2, matrix products, attend_block(): jnp.einsum('hgqk,khd->qhgd', weights, value_block, preferred_element_type...  10.1 us
    ppermute x5, starting transfers between devices, ring_weights(): left = lambda v: lax.ppermute(v, 'x', shifted(4, -1))  9.53 us
  transfers between devices with their start and end apart: 27, of which 10 were waited for; matrix products, arithmetic and copies ran while one was open for 11% of the time, Pallas kernels for 19%

profile of v1, /device:TPU:0, one launch (start us, length us, event | category | flops | bytes accessed | tf_op | source)
XLA Modules:
  0.0 305.2 jit_solution(6689676360962574272)
XLA Ops:
  7.2 0.6 pad_add_fusion.place
  7.8 5.1 %prep.1 = (bf16[128,2176]{1,0:T(8,128)(2,1)}, bf16[128,2176]{1,0:T(8,128)(2,1)}, bf16[128,2176]{1,0:T(8,128)(2,1)}, bf16[128,2176]{1,0:T(8,128)(2,1)}, bf16[512,512]{1,0:T(8,128)(2,1)}) custom-call(s32[2]{0:T(128)} %pad_add_fusion.place, bf16[512,2048]{1,0:T(8,128)(2,1)} %tok.1, s32[2,512]{1,0:T(2,128)} %bitcast.106, f32[2,512]{1,0:T(2,128)} %bitcast.107, ...), custom_call_target="tpu_custom_call" | custom-call | flops 6000000000 | bytes 6000000 | tf_op jit(solution)/shard_map/prep/pallas_call | solution.py:71
  13.0 4.0 %collective-permute-start.18 = (bf16[128,2176]{1,0:T(8,128)(2,1)}, bf16[128,2176]{1,0:T(8,128)(2,1)S(1)}, u32[]{:S(2)}, u32[]{:S(2)}) collective-permute-start(bf16[128,2176]{1,0:T(8,128)(2,1)} %get-tuple-element.101), channel_id=1, source_target_pairs={{0,64},{32,96},{64,0},{96,32},{1,65},{33,97},{65,1},{97,33},{2,66}... | collective-permute-start | bytes 1671176 | tf_op jit(solution)/shard_map/ppermute | solution.py:311
  16.9 0.7 collective-permute-start.17
  17.7 1.3 collective-permute-start.16
  19.0 11.7 %collective-permute-done.18 = bf16[128,2176]{1,0:T(8,128)(2,1)S(1)} collective-permute-done((bf16[128,2176]{1,0:T(8,128)(2,1)}, bf16[128,2176]{1,0:T(8,128)(2,1)S(1)}, u32[]{:S(2)}, u32[]{:S(2)}) %collective-permute-start.18) | collective-permute-done | bytes 557088 | tf_op jit(solution)/shard_map/ppermute | solution.py:311
  30.7 11.8 %collective-permute-done.17 = bf16[128,2176]{1,0:T(8,128)(2,1)S(1)} collective-permute-done((bf16[128,2176]{1,0:T(8,128)(2,1)}, bf16[128,2176]{1,0:T(8,128)(2,1)S(1)}, u32[]{:S(2)}, u32[]{:S(2)}) %collective-permute-start.17) | collective-permute-done | bytes 557088 | tf_op jit(solution)/shard_map/ppermute | solution.py:311
  42.5 1.3 pad_maximum_fusion
  43.9 0.7 all-gather.5.cloned.1.call-update
  44.6 1.6 collective-permute-start.6
  46.2 1.7 collective-permute-start.10
  48.2 2.9 collective-permute-start.13
  51.5 20.6 %collective-permute-done.6.refs_1_ = bf16[2048,256]{1,0:T(8,128)(2,1)S(1)} collective-permute-done((bf16[2048,256]{1,0:T(8,128)(2,1)}, bf16[2048,256]{1,0:T(8,128)(2,1)S(1)}, u32[]{:S(2)}, u32[]{:S(2)}) %collective-permute-start.6) | collective-permute-done | bytes 1048608 | tf_op jit(solution)/shard_map/ppermute | solution.py:223
  72.4 1.5 collective-permute-start.8
  73.9 20.7 %collective-permute-done.12.refs_1_ = bf16[2048,256]{1,0:T(8,128)(2,1)S(1)} collective-permute-done((bf16[2048,256]{1,0:T(8,128)(2,1)S(1)}, bf16[2048,256]{1,0:T(8,128)(2,1)S(1)}, u32[]{:S(2)}, u32[]{:S(2)}) %collective-permute-start.12) | collective-permute-done | bytes 1048608 | tf_op jit(solution)/shard_map/ppermute | solution.py:223
  94.6 1.5 collective-permute-start.11
  96.2 0.8 slice.52
  97.5 0.8 slice.53
  98.3 19.0 %collective-permute-done.7.refs_2_ = bf16[2048,256]{1,0:T(8,128)(2,1)S(1)} collective-permute-done((bf16[2048,256]{1,0:T(8,128)(2,1)}, bf16[2048,256]{1,0:T(8,128)(2,1)S(1)}, u32[]{:S(2)}, u32[]{:S(2)}) %collective-permute-start.7) | collective-permute-done | bytes 1048608 | tf_op jit(solution)/shard_map/ppermute | solution.py:224
  117.4 3.0 collective-permute-start.15
  120.3 19.2 %collective-permute-done.8.refs_3_ = bf16[2048,256]{1,0:T(8,128)(2,1)S(1)} collective-permute-done((bf16[2048,256]{1,0:T(8,128)(2,1)S(1)}, bf16[2048,256]{1,0:T(8,128)(2,1)S(1)}, u32[]{:S(2)}, u32[]{:S(2)}) %collective-permute-start.8) | collective-permute-done | bytes 1048608 | tf_op jit(solution)/shard_map/ppermute | solution.py:223
  139.6 1.0 copy-done.16
  140.6 21.9 %hidden.3 = bf16[1536,1024]{1,0:T(8,128)(2,1)} custom-call(s32[2]{0:T(128)} %pad_add_fusion.place, bf16[24,128,2176]{2,1,0:T(8,128)(2,1)} %bitcast.103, bf16[2048,256]{1,0:T(8,128)(2,1)} %bitcast.24.refs_0_, bf16[2048,256]{1,0:T(8,128)(2,1)} %copy-done.12, bf16[2048,256]{1,0:T(8,128)(2,1)} %copy-done.14, bf16[2048,256]{1,0:T(8,128)(2,1)} %copy-done.16, ...), custom_call_target="tpu_custom_call" | custom-call | flops 12884901888 | bytes 21369344 | tf_op jit(solution)/shard_map/hidden/pallas_call | solution.py:133
  162.5 0.8 copy-done.5
  163.2 0.8 copy-done.6
  164.1 15.4 %result.3 = bf16[3072,2048]{1,0:T(8,128)(2,1)} custom-call(s32[2]{0:T(128)} %pad_add_fusion.place, bf16[24,128,2176]{2,1,0:T(8,128)(2,1)} %bitcast.104, bf16[1536,1024]{1,0:T(8,128)(2,1)} %hidden.3, bf16[2048,256]{1,0:T(8,128)(2,1)} %bitcast.96, bf16[2048,256]{1,0:T(8,128)(2,1)} %copy-done.1, bf16[2048,256]{1,0:T(8,128)(2,1)} %copy-done.2, ...), custom_call_target="tpu_custom_call" | custom-call | flops 9663676416 | bytes 20582912 | tf_op jit(solution)/shard_map/result/pallas_call | solution.py:178
  179.5 0.8 copy-done.8
  180.4 1.3 collective-permute-start.1
  181.7 3.0 collective-permute-start
  184.8 2.4 collective-permute-start.3
  187.4 12.1 %hidden.2 = bf16[512,1024]{1,0:T(8,128)(2,1)} custom-call(s32[2]{0:T(128)} %pad_add_fusion.place, bf16[8,128,2176]{2,1,0:T(8,128)(2,1)} %bitcast.94, bf16[2048,256]{1,0:T(8,128)(2,1)} %bitcast.24.refs_0_, bf16[2048,256]{1,0:T(8,128)(2,1)} %copy-done.12, bf16[2048,256]{1,0:T(8,128)(2,1)} %copy-done.14, bf16[2048,256]{1,0:T(8,128)(2,1)} %copy-done.16, ...), custom_call_target="tpu_custom_call" | custom-call | flops 4294967296 | bytes 12456448 | tf_op jit(solution)/shard_map/hidden/pallas_call | solution.py:133
  199.5 8.3 %result.2 = bf16[1024,2048]{1,0:T(8,128)(2,1)} custom-call(s32[2]{0:T(128)} %pad_add_fusion.place, bf16[8,128,2176]{2,1,0:T(8,128)(2,1)} %bitcast.95, bf16[512,1024]{1,0:T(8,128)(2,1)} %hidden.2, bf16[2048,256]{1,0:T(8,128)(2,1)} %bitcast.97, bf16[2048,256]{1,0:T(8,128)(2,1)} %copy-done.1, bf16[2048,256]{1,0:T(8,128)(2,1)} %copy-done.2, ...), custom_call_target="tpu_custom_call" | custom-call | flops 3221225472 | bytes 12194304 | tf_op jit(solution)/shard_map/result/pallas_call | solution.py:178
  207.8 0.6 copy-done.10
  208.4 23.9 %while.12 = (s32[]{:T(128)}, bf16[2,512,256]{2,1,0:T(8,128)(2,1)}, s32[2]{0:T(128)S(1)}, bf16[1280,128]{0,1:T(8,128)(2,1)S(1)}, s32[]{:T(128)}, /*index=5*/bf16[...) while((s32[]{:T(128)}, bf16[2,512,256]{2,1,0:T(8,128)(2,1)}, ...), condition=%wide.region_3.4_spmd, body=%wide.region_0.3_spmd.sunk | while | flops 426778112 | bytes 47478112 | solution.py:283
  208.4 0.6 dynamic_slice.63
  209.7 0.8 fusion.50
  210.5 1.2 fusion.51
  211.8 1.6 fusion.52
  213.4 1.0 copy-done
  214.5 5.0 %fusion.53 = bf16[64,4,512]{2,0,1:T(8,128)(2,1)S(1)} fusion(f32[4,512]{1,0:T(4,128)S(1)} %exponential_add_fusion.2, f32[4,512]{1,0:T(4,128)S(1)} %broadcast_maximum_fusion.2, f32[768,512,4]{1,0,2:T(8,128)} %copy-done, pred[512,768]{0,1:T(8,128)(4,1)S(1)} %fusion.50, bf16[1280,128]{0,1:T(8,128)(2,1)S(1)} %get-tuple-element.209, s32[]{:T(128)S(6)} %select_n.102, ...), kind=kOutput, calls=%fused_computation.10.clone.1 | convolution fusion | flops 210894848 | bytes 7061512 | tf_op jit(solution)/shard_map/while/body/eval_jaxpr/hgqk,khd->qhgd/dot_general | solution.py:280
  219.7 0.7 constant_dynamic-update-slice_fusion.4
  220.4 0.6 dynamic_slice.63
  221.7 0.8 fusion.50
  222.5 1.2 fusion.51
  223.8 1.6 fusion.52
  225.4 1.0 copy-done
  226.4 5.0 %fusion.53 = bf16[64,4,512]{2,0,1:T(8,128)(2,1)S(1)} fusion(f32[4,512]{1,0:T(4,128)S(1)} %exponential_add_fusion.2, f32[4,512]{1,0:T(4,128)S(1)} %broadcast_maximum_fusion.2, f32[768,512,4]{1,0,2:T(8,128)} %copy-done, pred[512,768]{0,1:T(8,128)(4,1)S(1)} %fusion.50, bf16[1280,128]{0,1:T(8,128)(2,1)S(1)} %get-tuple-element.209, s32[]{:T(128)S(6)} %select_n.102, ...), kind=kOutput, calls=%fused_computation.10.clone.1 | convolution fusion | flops 210894848 | bytes 7061512 | tf_op jit(solution)/shard_map/while/body/eval_jaxpr/hgqk,khd->qhgd/dot_general | solution.py:280
  231.6 0.7 constant_dynamic-update-slice_fusion.4
  232.3 4.3 %all-to-all-start = ((bf16[4,256,256]{2,1,0:T(8,128)(2,1)}), bf16[4,256,256]{2,1,0:T(8,128)(2,1)S(1)}, u32[]{:S(2)}, u32[]{:S(2)}) async-start(bf16[4,256,256]{2,1,0:T(8,128)(2,1)} %bitcast.13), calls=%async_computation | async-start | bytes 1048576 | tf_op jit(solution)/shard_map/all_to_all | solution.py:321
  236.7 3.3 %collective-permute-start.5 = (bf16[128,2048]{1,0:T(8,128)(2,1)S(1)}, bf16[128,2048]{1,0:T(8,128)(2,1)S(1)}, u32[]{:S(2)}, u32[]{:S(2)}) collective-permute-start(bf16[128,2048]{1,0:T(8,128)(2,1)S(1)} %slice.51), channel_id=1, source_target_pairs={{0,3},{1,0},{2,1},{3,2},{4,7},{5,4},{6,5},{7,6},{8,11},{9,8},{10,9... | collective-permute-start | bytes 1572872 | tf_op jit(solution)/shard_map/ppermute | solution.py:325
  240.0 1.1 slice.50
  241.1 6.4 %all-to-all-done = bf16[4,256,256]{2,1,0:T(8,128)(2,1)S(1)} async-done(((bf16[4,256,256]{2,1,0:T(8,128)(2,1)}), bf16[4,256,256]{2,1,0:T(8,128)(2,1)S(1)}, u32[]{:S(2)}, u32[]{:S(2)}) %all-to-all-start) | async-done | bytes 524320 | tf_op jit(solution)/shard_map/all_to_all | solution.py:321
  247.5 1.9 fusion.26
  249.4 1.7 convolution_add_fusion.1
  251.1 5.1 %collective-permute-done.5 = bf16[128,2048]{1,0:T(8,128)(2,1)S(1)} collective-permute-done((bf16[128,2048]{1,0:T(8,128)(2,1)S(1)}, bf16[128,2048]{1,0:T(8,128)(2,1)S(1)}, u32[]{:S(2)}, u32[]{:S(2)}) %collective-permute-start.5) | collective-permute-done | bytes 524320 | tf_op jit(solution)/shard_map/ppermute | solution.py:325
  256.3 1.4 collective-permute-done.4
  257.7 1.5 fusion.19
  259.2 1.5 multiply_reduce_fusion
  260.7 2.3 fusion.37
  263.0 3.0 collective-permute-start.19
  266.4 0.9 collective-permute-start.21
  267.4 1.2 multiply_convert_fusion
  268.6 24.7 %reduce-scatter.3.cloned.1.call-done.first = bf16[128,2048]{1,0:T(8,128)(2,1)} async-done(((bf16[1024,2048]{1,0:T(8,128)(2,1)}), bf16[128,2048]{1,0:T(8,128)(2,1)}) %reduce-scatter.3.cloned.1.call-update) | async-done | bytes 524304 | tf_op jit(solution)/shard_map/reduce_scatter | solution.py:341
  293.3 5.4 %finish.1 = bf16[512,2048]{1,0:T(8,128)(2,1)} custom-call(bf16[512,512]{1,0:T(8,128)(2,1)} %get-tuple-element.97.order, bf16[128,2048]{1,0:T(8,128)(2,1)} %reduce-scatter.3.cloned.1.call-done.first, bf16[128,2048]{1,0:T(8,128)(2,1)} %collective-permute-done.19.second, bf16[128,2048]{1,0:T(8,128)(2,1)} %collective-permute-done.20.third, ...), custom_call_target="tpu_custom_call" | custom-call | flops 2000000000 | bytes 5000000 | tf_op jit(solution)/shard_map/finish/pallas_call | solution.py:211
  (81 shorter events, 3.2 us)
Async XLA Ops:
  7.2 133.4 %all-gather.7.cloned.1.call-start = ((), (), s32[]{:S(2)}) async-start(), calls=%async_computation.6 | async-start | bytes 15040512 | tf_op jit(solution)/shard_map/all_gather | solution.py:313
  13.0 35.0 %copy-start.4 = (bf16[1,2048,256]{2,1,0:T(8,128)(2,1)S(1)}, bf16[1,2048,256]{2,1,0:T(8,128)(2,1)}, u32[]{:S(2)}) copy-start(bf16[1,2048,256]{2,1,0:T(8,128)(2,1)} %param.27) | copy-start | bytes 3145732
  13.0 17.7 %collective-permute-start.18 = (bf16[128,2176]{1,0:T(8,128)(2,1)}, bf16[128,2176]{1,0:T(8,128)(2,1)S(1)}, u32[]{:S(2)}, u32[]{:S(2)}) collective-permute-start(bf16[128,2176]{1,0:T(8,128)(2,1)} %get-tuple-element.101), channel_id=1, source_target_pairs={{0,64},{32,96},{64,0},{96,32},{1,65},{33,97},{65,1},{97,33},{2,66}... | collective-permute-start | bytes 1671176 | tf_op jit(solution)/shard_map/ppermute | solution.py:311
  16.9 25.5 %collective-permute-start.17 = (bf16[128,2176]{1,0:T(8,128)(2,1)}, bf16[128,2176]{1,0:T(8,128)(2,1)S(1)}, u32[]{:S(2)}, u32[]{:S(2)}) collective-permute-start(bf16[128,2176]{1,0:T(8,128)(2,1)} %get-tuple-element.100), channel_id=1, source_target_pairs={{0,96},{32,0},{64,32},{96,64},{1,97},{33,1},{65,33},{97,65},{2,98}... | collective-permute-start | bytes 1671176 | tf_op jit(solution)/shard_map/ppermute | solution.py:311
  17.7 24.8 %collective-permute-start.16 = (bf16[128,2176]{1,0:T(8,128)(2,1)}, bf16[128,2176]{1,0:T(8,128)(2,1)S(1)}, u32[]{:S(2)}, u32[]{:S(2)}) collective-permute-start(bf16[128,2176]{1,0:T(8,128)(2,1)} %get-tuple-element.99), channel_id=1, source_target_pairs={{0,32},{32,64},{64,96},{96,0},{1,33},{33,65},{65,97},{97,1},{2,34}... | collective-permute-start | bytes 1671176 | tf_op jit(solution)/shard_map/ppermute | solution.py:311
  43.8 143.6 %all-gather.5.cloned.1.call-start = ((), (), s32[]{:S(2)}) async-start(), calls=%async_computation.5 | async-start | bytes 5013504 | tf_op jit(solution)/shard_map/all_gather | solution.py:312
  44.6 216.2 %reduce-scatter.5.cloned.1.call-start = ((), (), s32[]{:S(2)}) async-start(), calls=%async_computation.4 | async-start | bytes 14155776 | tf_op jit(solution)/shard_map/reduce_scatter | solution.py:340
  44.6 27.5 %collective-permute-start.6 = (bf16[2048,256]{1,0:T(8,128)(2,1)}, bf16[2048,256]{1,0:T(8,128)(2,1)S(1)}, u32[]{:S(2)}, u32[]{:S(2)}) collective-permute-start(bf16[2048,256]{1,0:T(8,128)(2,1)} %bitcast.24.refs_0_), channel_id=1, source_target_pairs={{0,1},{1,2},{2,3},{3,0},{4,5},{5,6},{6,7},{7,4},{8,9},{9,10},{10,1... | collective-permute-start | bytes 3145736 | tf_op jit(solution)/shard_map/ppermute | solution.py:223
  46.2 26.2 %collective-permute-start.10 = (bf16[2048,256]{1,0:T(8,128)(2,1)}, bf16[2048,256]{1,0:T(8,128)(2,1)S(1)}, u32[]{:S(2)}, u32[]{:S(2)}) collective-permute-start(bf16[2048,256]{1,0:T(8,128)(2,1)} %bitcast.25.refs_4_), channel_id=1, source_target_pairs={{0,3},{1,0},{2,1},{3,2},{4,7},{5,4},{6,5},{7,6},{8,11},{9,8},{10,9... | collective-permute-start | bytes 3145736 | tf_op jit(solution)/shard_map/ppermute | solution.py:224
  47.9 46.7 %collective-permute-start.12 = (bf16[2048,256]{1,0:T(8,128)(2,1)S(1)}, bf16[2048,256]{1,0:T(8,128)(2,1)S(1)}, u32[]{:S(2)}, u32[]{:S(2)}) collective-permute-start(bf16[2048,256]{1,0:T(8,128)(2,1)S(1)} %bitcast.98), channel_id=1, source_target_pairs={{0,1},{1,2},{2,3},{3,0},{4,5},{5,6},{6,7},{7,4},{8,9},{9,10},{10,1... | collective-permute-start | bytes 3145736 | tf_op jit(solution)/shard_map/ppermute | solution.py:223
  48.2 48.8 %collective-permute-start.13 = (bf16[2048,256]{1,0:T(8,128)(2,1)S(1)}, bf16[2048,256]{1,0:T(8,128)(2,1)S(1)}, u32[]{:S(2)}, u32[]{:S(2)}) collective-permute-start(bf16[2048,256]{1,0:T(8,128)(2,1)S(1)} %bitcast.99), channel_id=1, source_target_pairs={{0,3},{1,0},{2,1},{3,2},{4,7},{5,4},{6,5},{7,6},{8,11},{9,8},{10,9... | collective-permute-start | bytes 3145736 | tf_op jit(solution)/shard_map/ppermute | solution.py:224
  51.2 66.2 %collective-permute-start.7 = (bf16[2048,256]{1,0:T(8,128)(2,1)}, bf16[2048,256]{1,0:T(8,128)(2,1)S(1)}, u32[]{:S(2)}, u32[]{:S(2)}) collective-permute-start(bf16[2048,256]{1,0:T(8,128)(2,1)} %bitcast.24.refs_0_), channel_id=1, source_target_pairs={{0,3},{1,0},{2,1},{3,2},{4,7},{5,4},{6,5},{7,6},{8,11},{9,8},{10,9... | collective-permute-start | bytes 3145736 | tf_op jit(solution)/shard_map/ppermute | solution.py:224
  72.1 26.2 %copy-start.12 = (bf16[2048,256]{1,0:T(8,128)(2,1)}, bf16[2048,256]{1,0:T(8,128)(2,1)S(1)}, u32[]{:S(2)}) copy-start(bf16[2048,256]{1,0:T(8,128)(2,1)S(1)} %collective-permute-done.6.refs_1_) | copy-start | bytes 3145732
  72.1 48.2 %collective-permute-start.9 = (bf16[2048,256]{1,0:T(8,128)(2,1)}, bf16[2048,256]{1,0:T(8,128)(2,1)S(1)}, u32[]{:S(2)}, u32[]{:S(2)}) collective-permute-start(bf16[2048,256]{1,0:T(8,128)(2,1)} %bitcast.25.refs_4_), channel_id=1, source_target_pairs={{0,1},{1,2},{2,3},{3,0},{4,5},{5,6},{6,7},{7,4},{8,9},{9,10},{10,1... | collective-permute-start | bytes 3145736 | tf_op jit(solution)/shard_map/ppermute | solution.py:223
  72.4 67.1 %copy-start.13 = (bf16[2048,256]{1,0:T(8,128)(2,1)}, bf16[2048,256]{1,0:T(8,128)(2,1)S(1)}, u32[]{:S(2)}) copy-start(bf16[2048,256]{1,0:T(8,128)(2,1)S(1)} %collective-permute-done.10.refs_6_) | copy-start | bytes 3145732
  72.4 67.1 %collective-permute-start.8 = (bf16[2048,256]{1,0:T(8,128)(2,1)S(1)}, bf16[2048,256]{1,0:T(8,128)(2,1)S(1)}, u32[]{:S(2)}, u32[]{:S(2)}) collective-permute-start(bf16[2048,256]{1,0:T(8,128)(2,1)S(1)} %collective-permute-done.6.refs_1_), channel_id=1, source_target_pairs={{0,1},{1,2},{2,3},{3,0},{4,5},{5,6},{6,7},{7,4},{8,9},{9,10},{10,1... | collective-permute-start | bytes 3145736 | tf_op jit(solution)/shard_map/ppermute | solution.py:223
  94.6 67.8 %copy-start.1 = (bf16[2048,256]{1,0:T(8,128)(2,1)}, bf16[2048,256]{1,0:T(8,128)(2,1)S(1)}, u32[]{:S(2)}) copy-start(bf16[2048,256]{1,0:T(8,128)(2,1)S(1)} %collective-permute-done.12.refs_1_) | copy-start | bytes 3145732
  94.6 46.0 %collective-permute-start.11 = (bf16[2048,256]{1,0:T(8,128)(2,1)S(1)}, bf16[2048,256]{1,0:T(8,128)(2,1)}, u32[]{:S(2)}, u32[]{:S(2)}) collective-permute-start(bf16[2048,256]{1,0:T(8,128)(2,1)S(1)} %collective-permute-done.10.refs_6_), channel_id=1, source_target_pairs={{0,3},{1,0},{2,1},{3,2},{4,7},{5,4},{6,5},{7,6},{8,11},{9,8},{10,9... | collective-permute-start | bytes 3145736 | tf_op jit(solution)/shard_map/ppermute | solution.py:224
  97.0 65.4 %copy-start.2 = (bf16[2048,256]{1,0:T(8,128)(2,1)}, bf16[2048,256]{1,0:T(8,128)(2,1)S(1)}, u32[]{:S(2)}) copy-start(bf16[2048,256]{1,0:T(8,128)(2,1)S(1)} %collective-permute-done.13.refs_2_) | copy-start | bytes 3145732
  97.0 65.5 %collective-permute-start.14 = (bf16[1024,256]{1,0:T(8,128)(2,1)}, bf16[1024,256]{1,0:T(8,128)(2,1)S(1)}, u32[]{:S(2)}, u32[]{:S(2)}) collective-permute-start(bf16[1024,256]{1,0:T(8,128)(2,1)} %slice.52), channel_id=1, source_target_pairs={{0,1},{1,2},{2,3},{3,0},{4,5},{5,6},{6,7},{7,4},{8,9},{9,10},{10,1... | collective-permute-start | bytes 1572872 | tf_op jit(solution)/shard_map/ppermute | solution.py:223
  117.4 22.2 %copy-start.14 = (bf16[2048,256]{1,0:T(8,128)(2,1)}, bf16[2048,256]{1,0:T(8,128)(2,1)S(1)}, u32[]{:S(2)}) copy-start(bf16[2048,256]{1,0:T(8,128)(2,1)S(1)} %collective-permute-done.7.refs_2_) | copy-start | bytes 3145732
  117.4 45.1 %collective-permute-start.15 = (bf16[1024,256]{1,0:T(8,128)(2,1)}, bf16[1024,256]{1,0:T(8,128)(2,1)S(1)}, u32[]{:S(2)}, u32[]{:S(2)}) collective-permute-start(bf16[1024,256]{1,0:T(8,128)(2,1)} %slice.53), channel_id=1, source_target_pairs={{0,3},{1,0},{2,1},{3,2},{4,7},{5,4},{6,5},{7,6},{8,11},{9,8},{10,9... | collective-permute-start | bytes 1572872 | tf_op jit(solution)/shard_map/ppermute | solution.py:224
  120.3 19.2 %copy-start.15 = (bf16[2048,256]{1,0:T(8,128)(2,1)}, bf16[2048,256]{1,0:T(8,128)(2,1)S(1)}, u32[]{:S(2)}) copy-start(bf16[2048,256]{1,0:T(8,128)(2,1)S(1)} %collective-permute-done.9.refs_5_) | copy-start | bytes 3145732
  139.6 1.0 copy-start.16
  162.4 0.8 copy-start.5
  163.2 0.8 copy-start.6
  179.4 0.9 copy-start.8
  179.4 1.0 copy-start.9
  179.4 7.7 %copy-start.7 = (bf16[1024,256]{1,0:T(8,128)(2,1)S(1)}, bf16[1024,256]{1,0:T(8,128)(2,1)}, u32[]{:S(2)}) copy-start(bf16[1024,256]{1,0:T(8,128)(2,1)} %param.15) | copy-start | bytes 1572868
  179.5 113.9 %reduce-scatter.3.cloned.1.call-start = ((), (), s32[]{:S(2)}) async-start(), calls=%async_computation.3 | async-start | bytes 4718592 | tf_op jit(solution)/shard_map/reduce_scatter | solution.py:341
  180.4 6.9 %collective-permute-start.1 = (bf16[128,128]{0,1:T(8,128)(2,1)S(1)}, bf16[128,128]{0,1:T(8,128)(2,1)S(1)}, u32[]{:S(2)}, u32[]{:S(2)}) collective-permute-start(bf16[128,128]{0,1:T(8,128)(2,1)S(1)} %get-tuple-element.124), channel_id=1, source_target_pairs={{4,0},{8,4},{12,8},{16,12},{20,16},{24,20},{28,24},{32,28},{36,32}... | collective-permute-start | bytes 98312 | tf_op jit(solution)/shard_map/ppermute | solution.py:247
  181.7 5.6 %collective-permute-start = (bf16[128,128]{0,1:T(8,128)(2,1)S(1)}, bf16[128,128]{0,1:T(8,128)(2,1)S(1)}, u32[]{:S(2)}, u32[]{:S(2)}) collective-permute-start(bf16[128,128]{0,1:T(8,128)(2,1)S(1)} %get-tuple-element.123), channel_id=1, source_target_pairs={{0,4},{4,8},{8,12},{12,16},{16,20},{20,24},{24,28},{28,32},{32,36}... | collective-permute-start | bytes 98312 | tf_op jit(solution)/shard_map/ppermute | solution.py:246
  184.8 51.9 %collective-permute-start.3 = (bf16[256,2048]{1,0:T(8,128)(2,1)}, bf16[256,2048]{1,0:T(8,128)(2,1)S(1)}, u32[]{:S(2)}, u32[]{:S(2)}) collective-permute-start(bf16[256,2048]{1,0:T(8,128)(2,1)} %param.19), channel_id=1, source_target_pairs={{0,3},{1,0},{2,1},{3,2},{4,7},{5,4},{6,5},{7,6},{8,11},{9,8},{10,9... | collective-permute-start | bytes 3145736 | tf_op jit(solution)/shard_map/ppermute | solution.py:323
  187.1 52.9 %collective-permute-start.2 = (bf16[256,2048]{1,0:T(8,128)(2,1)}, bf16[256,2048]{1,0:T(8,128)(2,1)}, u32[]{:S(2)}, u32[]{:S(2)}) collective-permute-start(bf16[256,2048]{1,0:T(8,128)(2,1)} %param.19), channel_id=1, source_target_pairs={{0,1},{1,2},{2,3},{3,0},{4,5},{5,6},{6,7},{7,4},{8,9},{9,10},{10,1... | collective-permute-start | bytes 3145736 | tf_op jit(solution)/shard_map/ppermute | solution.py:322
  207.8 0.7 copy-start.10
  211.7 2.7 copy-start
  223.7 2.7 copy-start
  232.3 15.2 %all-to-all-start = ((bf16[4,256,256]{2,1,0:T(8,128)(2,1)}), bf16[4,256,256]{2,1,0:T(8,128)(2,1)S(1)}, u32[]{:S(2)}, u32[]{:S(2)}) async-start(bf16[4,256,256]{2,1,0:T(8,128)(2,1)} %bitcast.13), calls=%async_computation | async-start | bytes 1048576 | tf_op jit(solution)/shard_map/all_to_all | solution.py:321
  236.7 19.6 %collective-permute-start.5 = (bf16[128,2048]{1,0:T(8,128)(2,1)S(1)}, bf16[128,2048]{1,0:T(8,128)(2,1)S(1)}, u32[]{:S(2)}, u32[]{:S(2)}) collective-permute-start(bf16[128,2048]{1,0:T(8,128)(2,1)S(1)} %slice.51), channel_id=1, source_target_pairs={{0,3},{1,0},{2,1},{3,2},{4,7},{5,4},{6,5},{7,6},{8,11},{9,8},{10,9... | collective-permute-start | bytes 1572872 | tf_op jit(solution)/shard_map/ppermute | solution.py:325
  241.1 16.6 %collective-permute-start.4 = (bf16[128,2048]{1,0:T(8,128)(2,1)S(1)}, bf16[128,2048]{1,0:T(8,128)(2,1)}, u32[]{:S(2)}, u32[]{:S(2)}) collective-permute-start(bf16[128,2048]{1,0:T(8,128)(2,1)S(1)} %slice.50), channel_id=1, source_target_pairs={{0,1},{1,2},{2,3},{3,0},{4,5},{5,6},{6,7},{7,4},{8,9},{9,10},{10,1... | collective-permute-start | bytes 1572872 | tf_op jit(solution)/shard_map/ppermute | solution.py:325
  247.5 10.2 %copy-start.3 = (bf16[4,256,256]{2,1,0:T(8,128)(2,1)}, bf16[4,256,256]{2,1,0:T(8,128)(2,1)S(1)}, u32[]{:S(2)}) copy-start(bf16[4,256,256]{2,1,0:T(8,128)(2,1)S(1)} %all-to-all-done) | copy-start | bytes 1572868
  260.7 6.7 %copy-start.11 = (f32[2048]{0:T(1024)S(1)}, f32[2048]{0:T(1024)}, u32[]{:S(2)}) copy-start(f32[2048]{0:T(1024)} %param.20) | copy-start | bytes 24580
  263.0 30.3 %collective-permute-start.19 = (bf16[128,2048]{1,0:T(8,128)(2,1)}, bf16[128,2048]{1,0:T(8,128)(2,1)}, u32[]{:S(2)}, u32[]{:S(2)}) collective-permute-start(bf16[128,2048]{1,0:T(8,128)(2,1)} %get-tuple-element.122), channel_id=1, source_target_pairs={{0,96},{32,0},{64,32},{96,64},{1,97},{33,1},{65,33},{97,65},{2,98}... | collective-permute-start | bytes 1572872 | tf_op jit(solution)/shard_map/ppermute | solution.py:344
  266.1 27.3 %collective-permute-start.20 = (bf16[128,2048]{1,0:T(8,128)(2,1)S(1)}, bf16[128,2048]{1,0:T(8,128)(2,1)}, u32[]{:S(2)}, u32[]{:S(2)}) collective-permute-start(bf16[128,2048]{1,0:T(8,128)(2,1)S(1)} %get-tuple-element.121), channel_id=1, source_target_pairs={{0,64},{32,96},{64,0},{96,32},{1,65},{33,97},{65,1},{97,33},{2,66}... | collective-permute-start | bytes 1572872 | tf_op jit(solution)/shard_map/ppermute | solution.py:344
  266.4 26.9 %collective-permute-start.21 = (bf16[128,2048]{1,0:T(8,128)(2,1)S(1)}, bf16[128,2048]{1,0:T(8,128)(2,1)}, u32[]{:S(2)}, u32[]{:S(2)}) collective-permute-start(bf16[128,2048]{1,0:T(8,128)(2,1)S(1)} %get-tuple-element.120), channel_id=1, source_target_pairs={{0,32},{32,64},{64,96},{96,0},{1,33},{33,65},{65,97},{97,1},{2,34}... | collective-permute-start | bytes 1572872 | tf_op jit(solution)/shard_map/ppermute | solution.py:344
Sparse Core Ops, SparseCore 0:
  43.9 71.5 all-gather.6
  117.2 33.5 all-gather.4
  179.6 72.5 reduce-scatter.4
  254.5 38.8 reduce-scatter.2
